TPU v7x, 32 devices: a whole 2x2x4 slice. The times are simulated.
32 devices in a mesh: dp: 4 (over y, x), kv: 4 (over z), tp: 2 (over core).
Axes of the slice: x: 2, y: 2, z: 4, core: 2. Of those that a mesh axis runs over, the one named last changes fastest.
Arguments:
- stream: bfloat16 [32, 2048], P('dp', ('kv', 'tp')), parts along dimension 0, may hold values from -40 to 40
- old_state: float32 [32, 8, 64, 128], P(('dp', 'kv'), 'tp'), parts along dimension 0, may hold values from -6 to 6
- decay_amounts: float32 [32, 512], P(('dp', 'kv'), 'tp'), parts along dimension 0, may hold values from 0.003 to 1
- first_gain: float32 [2048], replicated, may hold values from 0.1 to 1.9
- first_gate: bfloat16 [2048, 5632], P(None, ('kv', 'tp')), may hold values from -0.125 to 0.125
- first_up: bfloat16 [2048, 5632], P(None, ('kv', 'tp')), may hold values from -0.125 to 0.125
- first_down: bfloat16 [5632, 2048], P(('kv', 'tp')), may hold values from -0.078125 to 0.078125
- mixer_gain: float32 [2048], P('kv'), may hold values from 0.1 to 1.9
- query_weight: bfloat16 [2048, 512], P('kv', 'tp'), may hold values from -0.125 to 0.125
- key_weight: bfloat16 [2048, 512], P('kv', 'tp'), may hold values from -0.125 to 0.125
- decay_weight: bfloat16 [2048, 512], P('kv', 'tp'), may hold values from -0.5 to 0.5
- value_weight: bfloat16 [2048, 1024], P('kv', 'tp'), may hold values from -0.125 to 0.125
- output_gate_weight: bfloat16 [2048, 1024], P('kv', 'tp'), may hold values from -0.125 to 0.125
- head_gain: float32 [1024], P('tp'), may hold values from 0.1 to 1.9
- output_weight: bfloat16 [1024, 2048], P('tp', 'kv'), may hold values from -0.1875 to 0.1875
- second_gain: float32 [2048], replicated, may hold values from 0.1 to 1.9
- second_gate: bfloat16 [2048, 5632], P(None, ('kv', 'tp')), may hold values from -0.125 to 0.125
- second_up: bfloat16 [2048, 5632], P(None, ('kv', 'tp')), may hold values from -0.125 to 0.125
- second_down: bfloat16 [5632, 2048], P(('kv', 'tp')), may hold values from -0.078125 to 0.078125
Outputs:
- mixed_stream: bfloat16 [32, 2048], P('dp', ('kv', 'tp')), parts along dimension 0
- new_state: float32 [32, 8, 64, 128], P(('dp', 'kv'), 'tp'), parts along dimension 0
There are 4 independent parts, one for each index of `dp`. A program takes and returns all parts, laid end to end along the dimension named above; an argument that names none is the same for every part. Nothing has to cross between parts.
All inputs are finite; a program needn't handle non-finite values.
Results may differ from a plain program's by a relative error of at most 0.007.
Values may be sent and summed in bfloat16 or wider, within the bound.
A program may use at most 64 MiB of HBM per device.

v0:
```python
import jax
import jax.numpy as jnp
from jax import lax
from jax.sharding import PartitionSpec as P

D = 2048


EPSILON = 1e-06
GATE_SOFTNESS = 16.0


def half_block(stream, norm_gain, w_gate, w_up, w_down):
    wide = lax.all_gather(stream, ("kv", "tp"), axis=1, tiled=True).astype(jnp.float32)
    scaled = (wide * norm_gain).astype(jnp.bfloat16)
    gate_acc = jnp.dot(scaled, w_gate, preferred_element_type=jnp.float32)
    up_acc = jnp.dot(scaled, w_up, preferred_element_type=jnp.float32)
    square_acc = jnp.sum(wide * wide, axis=1)
    row_scale = lax.rsqrt(square_acc / norm_gain.shape[0] + EPSILON)[:, None]
    hidden = (jax.nn.silu(gate_acc * row_scale) * (up_acc * row_scale)).astype(jnp.bfloat16)
    partial_out = jnp.dot(hidden, w_down, preferred_element_type=jnp.float32)
    summed = lax.psum_scatter(partial_out, ("kv", "tp"), scatter_dimension=1, tiled=True)
    return (stream.astype(jnp.float32) + 0.5 * summed).astype(jnp.bfloat16)


def body(
    stream,
    old_state,
    decay_amounts,
    first_gain,
    first_gate,
    first_up,
    first_down,
    mixer_gain,
    query_weight,
    key_weight,
    decay_weight,
    value_weight,
    output_gate_weight,
    head_gain,
    output_weight,
    second_gain,
    second_gate,
    second_up,
    second_down,
):
    middle = half_block(stream, first_gain, first_gate, first_up, first_down)
    paired_cols = lax.all_gather(middle, "tp", axis=1, tiled=True)
    wide_cols = paired_cols.astype(jnp.float32)
    scaled = (wide_cols * mixer_gain).astype(jnp.bfloat16)
    query_part = jnp.dot(scaled, query_weight, preferred_element_type=jnp.float32)
    key_part = jnp.dot(scaled, key_weight, preferred_element_type=jnp.float32)
    decay_part = jnp.dot(scaled, decay_weight, preferred_element_type=jnp.float32)
    value_part = jnp.dot(scaled, value_weight, preferred_element_type=jnp.float32)
    outgate_part = jnp.dot(scaled, output_gate_weight, preferred_element_type=jnp.float32)
    local_rows = old_state.shape[0]
    local_heads = old_state.shape[1]
    key_dim = old_state.shape[2]
    value_dim = old_state.shape[3]
    query_sum, key_sum, decay_sum, value_sum, outgate_sum, own_squares = (
        lax.psum_scatter(query_part, "kv", scatter_dimension=0, tiled=True),
        lax.psum_scatter(key_part, "kv", scatter_dimension=0, tiled=True),
        lax.psum_scatter(decay_part, "kv", scatter_dimension=0, tiled=True),
        lax.psum_scatter(value_part, "kv", scatter_dimension=0, tiled=True),
        lax.psum_scatter(outgate_part, "kv", scatter_dimension=0, tiled=True),
        lax.psum_scatter(
            jnp.sum(wide_cols * wide_cols, axis=1), "kv", scatter_dimension=0, tiled=True
        ),
    )
    row_scale = lax.rsqrt(own_squares / D + EPSILON)[:, None]
    query = (query_sum * row_scale * key_dim ** (-0.5)).reshape(local_rows, local_heads, key_dim)
    keys = (key_sum * row_scale).reshape(local_rows, local_heads, key_dim)
    gate_logits = (decay_sum * row_scale).reshape(local_rows, local_heads, key_dim)
    values = (value_sum * row_scale).reshape(local_rows, local_heads, value_dim)
    decay_logarithm = jax.nn.log_sigmoid(gate_logits) / GATE_SOFTNESS - decay_amounts.reshape(
        local_rows, local_heads, key_dim
    )
    new_state = (
        jnp.exp(decay_logarithm)[..., None] * old_state + keys[..., None] * values[:, :, None, :]
    )
    readout = jnp.einsum("bhk,bhkv->bhv", query, new_state, precision=lax.Precision.HIGHEST)
    normed = readout * lax.rsqrt(jnp.mean(readout * readout, axis=-1, keepdims=True) + EPSILON)
    mixed_heads = (
        normed.reshape(local_rows, local_heads * value_dim)
        * head_gain
        * jax.nn.silu(outgate_sum * row_scale)
    ).astype(jnp.bfloat16)
    projected = jnp.dot(
        lax.all_gather(mixed_heads, "kv", axis=0, tiled=True),
        output_weight,
        preferred_element_type=jnp.float32,
    ).astype(jnp.bfloat16)
    attention_out = lax.psum_scatter(
        lax.optimization_barrier(projected).astype(jnp.float32).astype(jnp.bfloat16),
        "tp",
        scatter_dimension=1,
        tiled=True,
    ).astype(jnp.float32)
    after = (middle.astype(jnp.float32) + attention_out).astype(jnp.bfloat16)
    mixed_stream = half_block(after, second_gain, second_gate, second_up, second_down)
    return (mixed_stream, new_state)


def solution(mesh):
    in_specs = (
        P("dp", ("kv", "tp")),
        P(("dp", "kv"), "tp", None, None),
        P(("dp", "kv"), "tp"),
        P(),
        P(None, ("kv", "tp")),
        P(None, ("kv", "tp")),
        P(("kv", "tp"), None),
        P("kv"),
        P("kv", "tp"),
        P("kv", "tp"),
        P("kv", "tp"),
        P("kv", "tp"),
        P("kv", "tp"),
        P("tp"),
        P("tp", "kv"),
        P(),
        P(None, ("kv", "tp")),
        P(None, ("kv", "tp")),
        P(("kv", "tp"), None),
    )
    out_specs = (P("dp", ("kv", "tp")), P(("dp", "kv"), "tp", None, None))
    return jax.shard_map(body, mesh=mesh, in_specs=in_specs, out_specs=out_specs, check_vma=False)
```

profile of v0, /device:TPU:0, one launch (start us, length us, event | category | flops | bytes accessed | tf_op | source)
XLA Modules:
  0.0 171.4 jit_solution(4641886258188548074)
XLA Ops:
  7.2 16.1 %all_gather.12 = bf16[8,2048]{1,0:T(8,128)(2,1)S(1)} all-gather(bf16[8,256]{1,0:T(8,128)(2,1)} %param.19), channel_id=1, replica_groups=mesh['dp'=4,'kv'=4,'tp'=2] {'kv','tp'}, dimensions={1}, use_global_device_ids=true | all-gather | bytes 36864 | tf_op jit(solution)/shard_map/all_gather | solution.py:14
  23.3 0.1 fusion.7
  23.4 2.7 %convolution_multiply_fusion.3 = f32[8,704]{1,0:T(8,128)S(1)} fusion(bf16[2048,704]{0,1:T(8,128)(2,1)} %param.23, bf16[8,2048]{1,0:T(8,128)(2,1)S(1)} %all_gather.12, f32[2048]{0:T(1024)} %param.22, f32[8]{0:T(128)S(1)} %add_rsqrt_fusion.2), kind=kOutput, calls=%fused_computation.5 | convolution fusion | flops 23123456 | bytes 2947104 | tf_op jit(solution)/shard_map/dot_general | solution.py:16
  26.2 4.2 %fusion.5 = f32[8,2048]{1,0:T(8,128)} fusion(bf16[704,2048]{1,0:T(8,128)(2,1)S(1)} %copy-done, bf16[2048,704]{0,1:T(8,128)(2,1)} %param.24, bf16[8,2048]{1,0:T(8,128)(2,1)S(1)} %all_gather.12, f32[2048]{0:T(1024)S(1)} %copy-done.4, f32[8,704]{1,0:T(8,128)S(1)} %convolution_multiply_fusion.3, f32[8]{0:T(128)S(1)} %add_rsqrt_fusion.2), kind=kOutput, calls=%fused_computation.9 | convolution fusion | flops 46225920 | bytes 5896224 | tf_op jit(solution)/shard_map/dot_general | solution.py:21
  30.5 0.1 reshape.62
  30.5 0.6 dynamic-slice
  31.1 30.9 %reduce-scatter.4.cloned.1.call-done = f32[8,256]{1,0:T(8,128)} async-done(((f32[8,2048]{1,0:T(8,128)}), f32[8,256]{1,0:T(8,128)}) %reduce-scatter.4.cloned.1.call-update) | async-done | bytes 8208 | tf_op jit(solution)/shard_map/reduce_scatter | solution.py:22
  62.0 0.7 add_convert_fusion.2
  62.7 1.8 %all_gather.13 = bf16[8,512]{1,0:T(8,128)(2,1)S(1)} all-gather(bf16[8,256]{1,0:T(8,128)(2,1)S(1)} %add_convert_fusion.2), channel_id=1, replica_groups=mesh['dp'=4,'kv'=4,'tp'=2] {'tp'}, dimensions={1}, use_global_device_ids=true | all-gather | bytes 12288 | tf_op jit(solution)/shard_map/all_gather | solution.py:48
  64.5 0.1 fusion.27
  64.7 1.1 fusion.49
  65.8 1.1 fusion.47
  66.9 1.1 fusion.51
  68.0 0.2 fusion.45
  68.1 1.2 fusion.43
  70.0 16.6 %all-reduce.6 = (f32[8]{0:T(128)S(1)}, f32[8,512]{1,0:T(8,128)S(1)}, f32[8,256]{1,0:T(8,128)S(1)}, f32[8,512]{1,0:T(8,128)S(1)}, f32[8,256]{1,0:T(8,128)S(1)}, /*index=5*/f32[8,256]{1,0:T(8,128)S(1)}) all-reduce(f32[8]{0:T(128)S(1)} %fusion.27, f32[8,512]{1,0:T(8,128)S(1)} %fusion.43, ...), channel_id=4, replica_groups=mesh['dp'=4,'kv'=4,'tp'=2] {'kv'}, use_global_device_ids=true, to_apply=%region_4.5.clone | all-reduce | flops 14344 | bytes 114752
  86.9 0.1 neg.41
  87.0 0.1 mul.191
  87.2 1.1 multiply_add_fusion
  88.4 0.3 fusion.55
  88.7 0.1 multiply_reduce_fusion
  88.8 0.1 fusion.40
  89.0 11.9 %all-gather = bf16[4,2,512]{2,1,0:T(2,128)(2,1)S(1)} all-gather(bf16[1,2,512]{2,1,0:T(2,128)(2,1)S(1)} %fusion.40), channel_id=1, replica_groups=mesh['dp'=4,'kv'=4,'tp'=2] {'kv'}, dimensions={0}, use_global_device_ids=true | all-gather | bytes 10240 | tf_op jit(solution)/shard_map/all_gather | solution.py:89
  100.9 1.8 %convolution_convert_fusion = bf16[8,512]{1,0:T(8,128)(2,1)} fusion(bf16[8,512]{1,0:T(8,128)(2,1)S(1)} %reshape.65, bf16[512,512]{1,0:T(8,128)(2,1)} %param.33), kind=kOutput, calls=%fused_computation.10 | convolution fusion | flops 4198400 | bytes 540672 | tf_op jit(solution)/shard_map/dot_general | solution.py:88
  102.8 6.4 %reduce-scatter.6.cloned.1.call-done = bf16[8,256]{1,0:T(8,128)(2,1)} async-done(((bf16[8,512]{1,0:T(8,128)(2,1)}), bf16[8,256]{1,0:T(8,128)(2,1)}) %reduce-scatter.6.cloned.1.call-update) | async-done | bytes 4112 | tf_op jit(solution)/shard_map/reduce_scatter | solution.py:93
  109.2 0.7 add_convert_fusion.1
  109.8 14.3 %all_gather.15 = bf16[8,2048]{1,0:T(8,128)(2,1)S(1)} all-gather(bf16[8,256]{1,0:T(8,128)(2,1)S(1)} %add_convert_fusion.1), channel_id=1, replica_groups=mesh['dp'=4,'kv'=4,'tp'=2] {'kv','tp'}, dimensions={1}, use_global_device_ids=true | all-gather | bytes 36864 | tf_op jit(solution)/shard_map/all_gather | solution.py:14
  124.2 0.1 fusion.9
  124.3 2.7 %convolution_multiply_fusion.1 = f32[8,704]{1,0:T(8,128)S(1)} fusion(bf16[2048,704]{0,1:T(8,128)(2,1)} %param.35, bf16[8,2048]{1,0:T(8,128)(2,1)S(1)} %all_gather.15, f32[2048]{0:T(1024)S(1)} %copy-done.5, f32[8]{0:T(128)S(1)} %add_rsqrt_fusion.1), kind=kOutput, calls=%fused_computation.2 | convolution fusion | flops 23123456 | bytes 2947104 | tf_op jit(solution)/shard_map/dot_general | solution.py:16
  127.0 5.0 %fusion.4 = f32[8,2048]{1,0:T(8,128)} fusion(bf16[704,2048]{1,0:T(8,128)(2,1)} %param.37, bf16[2048,704]{0,1:T(8,128)(2,1)} %param.36, bf16[8,2048]{1,0:T(8,128)(2,1)S(1)} %all_gather.15, f32[2048]{0:T(1024)S(1)} %copy-done.5, f32[8,704]{1,0:T(8,128)S(1)} %convolution_multiply_fusion.1, f32[8]{0:T(128)S(1)} %add_rsqrt_fusion.1), kind=kOutput, calls=%fused_computation.8 | convolution fusion | flops 46225920 | bytes 5896224 | tf_op jit(solution)/shard_map/dot_general | solution.py:21
  132.0 31.5 %reduce-scatter.8.cloned.1.call-done = f32[8,256]{1,0:T(8,128)} async-done(((f32[8,2048]{1,0:T(8,128)}), f32[8,256]{1,0:T(8,128)}) %reduce-scatter.8.cloned.1.call-update) | async-done | bytes 8208 | tf_op jit(solution)/shard_map/reduce_scatter | solution.py:22
  163.5 1.3 add_convert_fusion
  (37 shorter events, 0.7 us)
Async XLA Ops:
  7.2 19.0 %copy-start = (bf16[704,2048]{1,0:T(8,128)(2,1)S(1)}, bf16[704,2048]{1,0:T(8,128)(2,1)}, u32[]{:S(2)}) copy-start(bf16[704,2048]{1,0:T(8,128)(2,1)} %param.25) | copy-start | bytes 8650756
  7.2 18.9 %copy-start.4 = (f32[2048]{0:T(1024)S(1)}, f32[2048]{0:T(1024)}, u32[]{:S(2)}) copy-start(f32[2048]{0:T(1024)} %param.22) | copy-start | bytes 24580
  7.2 54.8 %reduce-scatter.4.cloned.1.call-start = ((), (), s32[]{:S(2)}) async-start(), calls=%async_computation.3 | async-start | bytes 73728 | tf_op jit(solution)/shard_map/reduce_scatter | solution.py:22
  26.1 4.3 %copy-start.7 = (f32[2,256]{1,0:T(2,128)S(1)}, f32[2,256]{1,0:T(2,128)}, u32[]{:S(2)}) copy-start(f32[2,256]{1,0:T(2,128)} %param.21) | copy-start | bytes 6148
  26.1 4.4 %copy-start.9 = (u32[32]{0:T(128)S(1)}, u32[32]{0:T(128)}, u32[]{:S(2)}) copy-start(u32[32]{0:T(128)} %constant.35) | copy-start | bytes 388
  26.2 35.9 %copy-start.6 = (bf16[8,256]{1,0:T(8,128)(2,1)S(1)}, bf16[8,256]{1,0:T(8,128)(2,1)}, u32[]{:S(2)}) copy-start(bf16[8,256]{1,0:T(8,128)(2,1)} %param.19) | copy-start | bytes 12292
  26.2 38.5 %copy-start.3 = (f32[512]{0:T(512)S(1)}, f32[512]{0:T(512)}, u32[]{:S(2)}) copy-start(f32[512]{0:T(512)} %param.26) | copy-start | bytes 6148
  26.2 41.8 %copy-start.2 = (bf16[512,512]{1,0:T(8,128)(2,1)S(1)}, bf16[512,512]{1,0:T(8,128)(2,1)}, u32[]{:S(2)}) copy-start(bf16[512,512]{1,0:T(8,128)(2,1)} %param.30) | copy-start | bytes 1572868
  30.4 58.5 %copy-start.8 = (f32[512]{0:T(512)S(1)}, f32[512]{0:T(512)}, u32[]{:S(2)}) copy-start(f32[512]{0:T(512)} %param.32) | copy-start | bytes 6148
  30.4 93.9 %copy-start.5 = (f32[2048]{0:T(1024)S(1)}, f32[2048]{0:T(1024)}, u32[]{:S(2)}) copy-start(f32[2048]{0:T(1024)} %param.34) | copy-start | bytes 24580
  30.4 78.8 %reduce-scatter.6.cloned.1.call-start = ((), (), s32[]{:S(2)}) async-start(), calls=%async_computation.4 | async-start | bytes 12288 | tf_op jit(solution)/shard_map/reduce_scatter | solution.py:93
  88.4 43.6 %copy-start.1 = (f32[2,4,64,128]{3,2,1,0:T(8,128)}, f32[2,4,64,128]{3,2,1,0:T(8,128)S(1)}, u32[]{:S(2)}) copy-start(f32[2,4,64,128]{3,2,1,0:T(8,128)S(1)} %multiply_add_fusion) | copy-start | bytes 786436
  102.7 60.8 %reduce-scatter.8.cloned.1.call-start = ((), (), s32[]{:S(2)}) async-start(), calls=%async_computation.5 | async-start | bytes 73728 | tf_op jit(solution)/shard_map/reduce_scatter | solution.py:22
Sparse Core Ops, SparseCore 0:
  30.5 31.4 reduce-scatter.3
  102.9 6.2 reduce-scatter.5
  132.1 31.3 reduce-scatter.7
where the time goes:
time: 172 us; the launch traced here: 171 us
  waiting for transfers between devices  68.8 us (40%)
  blocking collectives  60.8 us (35%)
  matrix products  21.3 us (12%)
  between operations  14.6 us (8%)
  other arithmetic  4.73 us (3%)
    reduce_scatter x2, waiting for transfers between devices, half_block(): lax.psum_scatter(partial_out, ('kv', 'tp'), scatter_dimension=1, tiled=True)  62.4 us
    all_gather x2, blocking collectives, half_block(): lax.all_gather(stream, ('kv', 'tp'), axis=1, tiled=True).astype(jnp.float32)  30.4 us
    unnamed x1, blocking collectives  16.6 us
    all_gather x1, blocking collectives, body(): lax.all_gather(mixed_heads, 'kv', axis=0, tiled=True)  11.9 us
    dot_general x2, matrix products, half_block(): partial_out = jnp.dot(hidden, w_down, preferred_element_type=jnp.float32)  9.16 us
    reduce_scatter x1, waiting for transfers between devices, body(): lax.psum_scatter(lax.optimization_barrier(projected).astype(jnp.float32)....  6.35 us
    dot_general x2, matrix products, half_block(): gate_acc = jnp.dot(scaled, w_gate, preferred_element_type=jnp.float32)  5.33 us
  transfers between devices with their start and end apart: 3, of which 3 were waited for; matrix products, arithmetic and copies ran while one was open for 0% of the time, Pallas kernels for 0%

commit v1 on v0

--- a/solution.py
+++ b/solution.py
@@ -1,13 +1,342 @@
+import functools
+
 import jax
 import jax.numpy as jnp
 from jax import lax
+from jax.experimental import pallas as pl
+from jax.experimental.pallas import tpu as pltpu
 from jax.sharding import PartitionSpec as P
-
-D = 2048
-
 
 EPSILON = 1e-06
 GATE_SOFTNESS = 16.0
+MESH = pl.DeviceIdType.MESH
+F32 = jnp.float32
+BF16 = jnp.bfloat16
+
+
+def dot(a, b):
+    return jnp.dot(a, b, preferred_element_type=F32)
+
+
+def layer_kernel(
+    n_kv,
+    n_tp,
+    stream_h,
+    state_h,
+    amounts_h,
+    gain1_h,
+    gate1_h,
+    up1_h,
+    down1_h,
+    mixgain_h,
+    query_h,
+    key_h,
+    decay_h,
+    value_h,
+    outgate_h,
+    headgain_h,
+    output_h,
+    gain2_h,
+    gate2_h,
+    up2_h,
+    down2_h,
+    out_ref,
+    newstate_h,
+    stream_v,
+    state_v,
+    amounts_v,
+    gain1_v,
+    gate1_v,
+    up1_v,
+    down1_v,
+    mixgain_v,
+    proj_v,
+    headgain_v,
+    output_v,
+    gain2_v,
+    gate2_v,
+    up2_v,
+    down2_v,
+    newstate_v,
+    wide_v,
+    down_out,
+    down_in,
+    middle_v,
+    proj_out,
+    proj_in,
+    mixed_v,
+    attn_v,
+    after_v,
+    last_out,
+    last_in,
+    load_sem,
+    store_sem,
+    a_send,
+    a_recv,
+    c_send,
+    c_recv,
+    d_send,
+    d_recv,
+    m_send,
+    m_recv,
+    e_send,
+    e_recv,
+    g_send,
+    g_recv,
+    h_send,
+    h_recv,
+):
+    z = lax.axis_index("kv")
+    c = lax.axis_index("tp")
+    me = z * n_tp + c
+    seqs, own_cols = stream_v.shape
+    chip_cols = own_cols * n_tp
+    width = chip_cols * n_kv
+    rows, heads, key_dim, value_dim = state_v.shape
+    key_cols = heads * key_dim
+    value_cols = heads * value_dim
+
+    loads = []
+
+    def load(src, dst):
+        copy = pltpu.make_async_copy(src, dst, load_sem.at[len(loads)])
+        copy.start()
+        loads.append(copy)
+        return copy
+
+    load_stream = load(stream_h, stream_v)
+    load_gain1 = load(gain1_h, gain1_v)
+    load_gate1 = load(gate1_h, gate1_v)
+    load_up1 = load(up1_h, up1_v)
+    load_down1 = load(down1_h, down1_v)
+
+    far = []
+    for j in range(n_kv - 1):
+        down_t = n_kv - 1 - j
+        low = jnp.where(down_t <= z, down_t - 1, down_t)
+        high = jnp.where(j >= z, j + 1, j)
+        far.append(jnp.where(z < n_kv // 2, low, high))
+    cores = [lax.rem(c + k, n_tp) for k in range(n_tp)]
+    peers = [(t, k) for t in far for k in cores] + [(z, k) for k in cores[1:]]
+
+    barrier = pltpu.get_barrier_semaphore()
+    for t, k in peers:
+        pl.semaphore_signal(barrier, inc=1, device_id={"kv": t, "tp": k}, device_id_type=MESH)
+    pl.semaphore_wait(barrier, len(peers))
+
+    sent = []
+
+    def send(src, dst, send_sem, recv_sem, t, k):
+        copy = pltpu.make_async_remote_copy(
+            src_ref=src,
+            dst_ref=dst,
+            send_sem=send_sem,
+            recv_sem=recv_sem,
+            device_id={"kv": t, "tp": k},
+            device_id_type=MESH,
+        )
+        copy.start()
+        sent.append(copy)
+
+    def arrived(ref, send_sem, recv_sem, t, k):
+        pltpu.make_async_remote_copy(
+            src_ref=ref,
+            dst_ref=ref,
+            send_sem=send_sem,
+            recv_sem=recv_sem,
+            device_id={"kv": t, "tp": k},
+            device_id_type=MESH,
+        ).wait_recv()
+
+    load_stream.wait()
+    for p, (t, k) in enumerate(peers):
+        send(stream_v, wide_v.at[me], a_send.at[p], a_recv.at[me], t, k)
+    wide_v[me] = stream_v[...]
+
+    load_state = load(state_h, state_v)
+    load_small = [load(amounts_h, amounts_v), load(headgain_h, headgain_v)]
+    load_mix = [load(mixgain_h, mixgain_v)]
+    at = 0
+    for ref in (query_h, key_h, decay_h, value_h, outgate_h):
+        load_mix.append(load(ref, proj_v.at[:, at : at + ref.shape[1]]))
+        at += ref.shape[1]
+    proj_cols = at
+    load_output = load(output_h, output_v)
+    load_second = [load(gain2_h, gain2_v), load(gate2_h, gate2_v), load(up2_h, up2_v)]
+    load_down2 = load(down2_h, down2_v)
+
+    load_gain1.wait()
+    load_gate1.wait()
+    load_up1.wait()
+    gate_acc = jnp.zeros((seqs, gate1_v.shape[1]), F32)
+    up_acc = jnp.zeros((seqs, up1_v.shape[1]), F32)
+    squares = jnp.zeros((seqs, 1), F32)
+    order = [(z, k) for k in cores] + [(t, k) for t in far[::-1] for k in cores]
+    for i, (t, k) in enumerate(order):
+        who = t * n_tp + k
+        if i:
+            arrived(wide_v.at[who], a_send.at[0], a_recv.at[who], t, k)
+        block = wide_v[who].astype(F32)
+        cols = pl.ds(pl.multiple_of(who * own_cols, own_cols), own_cols)
+        scaled = (block * gain1_v[:, cols]).astype(BF16)
+        squares += jnp.sum(block * block, axis=1, keepdims=True)
+        gate_acc += dot(scaled, gate1_v[cols, :])
+        up_acc += dot(scaled, up1_v[cols, :])
+    scale = lax.rsqrt(squares / width + EPSILON)
+    hidden = (jax.nn.silu(gate_acc * scale) * (up_acc * scale)).astype(BF16)
+
+    load_down1.wait()
+    for j, t in enumerate(far):
+        cols = pl.ds(pl.multiple_of(t * chip_cols, chip_cols), chip_cols)
+        down_out[j] = dot(hidden, down1_v[:, cols]).astype(BF16)
+        for i, k in enumerate(cores):
+            send(down_out.at[j], down_in.at[me], c_send.at[j * n_tp + i], c_recv.at[me], t, k)
+    cols = pl.ds(pl.multiple_of(z * chip_cols, chip_cols), chip_cols)
+    own = dot(hidden, down1_v[:, cols])
+    down_out[n_kv - 1] = own.astype(BF16)
+    for i, k in enumerate(cores[1:]):
+        send(
+            down_out.at[n_kv - 1],
+            down_in.at[me],
+            c_send.at[(n_kv - 1) * n_tp + i],
+            c_recv.at[me],
+            z,
+            k,
+        )
+    summed = own.astype(BF16).astype(F32)
+    for t, k in order[1:]:
+        who = t * n_tp + k
+        arrived(down_in.at[who], c_send.at[0], c_recv.at[who], t, k)
+        summed += down_in[who].astype(F32)
+    chip_stream = jnp.concatenate([wide_v[z * n_tp + i] for i in range(n_tp)], axis=1)
+    middle = (chip_stream.astype(F32) + 0.5 * summed).astype(BF16)
+    middle_v[z] = middle
+
+    for copy in load_mix:
+        copy.wait()
+    middle_wide = middle.astype(F32)
+    scaled = (middle_wide * mixgain_v[...]).astype(BF16)
+    part = dot(scaled, proj_v[...])
+    square_part = jnp.broadcast_to(
+        jnp.sum(middle_wide * middle_wide, axis=1, keepdims=True), (seqs, 128)
+    )
+    for j in range(n_kv):
+        proj_out[j, :, :proj_cols] = part[j * rows : (j + 1) * rows]
+        proj_out[j, :, proj_cols:] = square_part[j * rows : (j + 1) * rows]
+    for j, t in enumerate(far):
+        send(proj_out.at[t], proj_in.at[z], d_send.at[j], d_recv.at[z], t, c)
+    for j, t in enumerate(far):
+        send(middle_v.at[z], middle_v.at[z], m_send.at[j], m_recv.at[z], t, c)
+
+    total = proj_out[z]
+    for t in far[::-1]:
+        arrived(proj_in.at[t], d_send.at[0], d_recv.at[t], t, c)
+        total += proj_in[t]
+    scale = lax.rsqrt(total[:, proj_cols : proj_cols + 1] / width + EPSILON)
+    total = total[:, :proj_cols] * scale
+    query = total[:, :key_cols] * key_dim ** (-0.5)
+    keys = total[:, key_cols : 2 * key_cols]
+    logits = total[:, 2 * key_cols : 3 * key_cols]
+    values = total[:, 3 * key_cols : 3 * key_cols + value_cols]
+    outgate = total[:, 3 * key_cols + value_cols :]
+    for copy in load_small:
+        copy.wait()
+    log_sigmoid = jnp.minimum(logits, 0.0) - jnp.log(1.0 + jnp.exp(-jnp.abs(logits)))
+    decay = jnp.exp(log_sigmoid / GATE_SOFTNESS - amounts_v[...])
+    stacked = jnp.concatenate(
+        [query, keys, decay, jnp.zeros((128 - 3 * rows, key_cols), F32)], axis=0
+    )
+    turned = stacked.T
+    gated = headgain_v[...] * jax.nn.silu(outgate)
+    load_state.wait()
+    mixed_rows = []
+    for b in range(rows):
+        pieces = []
+        for h in range(heads):
+            span = slice(h * key_dim, (h + 1) * key_dim)
+            lane = slice(h * value_dim, (h + 1) * value_dim)
+            q_col = turned[span, b : b + 1]
+            k_col = turned[span, rows + b : rows + b + 1]
+            d_col = turned[span, 2 * rows + b : 2 * rows + b + 1]
+            new = d_col * state_v[b, h] + k_col * values[b : b + 1, lane]
+            newstate_v[b, h] = new
+            readout = jnp.sum(q_col * new, axis=0, keepdims=True)
+            normed = readout * lax.rsqrt(
+                jnp.mean(readout * readout, axis=1, keepdims=True) + EPSILON
+            )
+            pieces.append(normed * gated[b : b + 1, lane])
+        mixed_rows.append(jnp.concatenate(pieces, axis=1))
+    store = pltpu.make_async_copy(newstate_v, newstate_h, store_sem)
+
+    mixed_v[z] = jnp.concatenate(mixed_rows, axis=0).astype(BF16).astype(F32)
+    for j, t in enumerate(far):
+        send(mixed_v.at[z], mixed_v.at[z], e_send.at[j], e_recv.at[z], t, c)
+    store.start()
+    load_output.wait()
+    for t in far[::-1]:
+        arrived(mixed_v.at[t], e_send.at[0], e_recv.at[t], t, c)
+    mixed = jnp.concatenate([mixed_v[j] for j in range(n_kv)], axis=0).astype(BF16)
+    attn_v[me] = dot(mixed, output_v[...]).astype(BF16)
+
+    for p, (t, k) in enumerate(peers):
+        send(attn_v.at[me], attn_v.at[me], g_send.at[p], g_recv.at[me], t, k)
+    for copy in load_second:
+        copy.wait()
+    gate_acc = jnp.zeros((seqs, gate2_v.shape[1]), F32)
+    up_acc = jnp.zeros((seqs, up2_v.shape[1]), F32)
+    squares = jnp.zeros((seqs, 1), F32)
+    for t in [z] + far[::-1]:
+        if t is not z:
+            arrived(middle_v.at[t], m_send.at[0], m_recv.at[t], t, c)
+        attention = jnp.zeros((seqs, chip_cols), F32)
+        for k in cores:
+            who = t * n_tp + k
+            if not (t is z and k is cores[0]):
+                arrived(attn_v.at[who], g_send.at[0], g_recv.at[who], t, k)
+            attention += attn_v[who].astype(F32)
+        after = (middle_v[t].astype(F32) + attention).astype(BF16)
+        block = after.astype(F32)
+        if t is z:
+            for i in range(n_tp):
+                after_v[i] = block[:, i * own_cols : (i + 1) * own_cols]
+        cols = pl.ds(pl.multiple_of(t * chip_cols, chip_cols), chip_cols)
+        scaled = (block * gain2_v[:, cols]).astype(BF16)
+        squares += jnp.sum(block * block, axis=1, keepdims=True)
+        gate_acc += dot(scaled, gate2_v[cols, :])
+        up_acc += dot(scaled, up2_v[cols, :])
+    scale = lax.rsqrt(squares / width + EPSILON)
+    hidden = (jax.nn.silu(gate_acc * scale) * (up_acc * scale)).astype(BF16)
+
+    load_down2.wait()
+    for j, t in enumerate(far):
+        cols = pl.ds(pl.multiple_of(t * chip_cols, chip_cols), chip_cols)
+        piece = dot(hidden, down2_v[:, cols]).astype(BF16)
+        for k in range(n_tp):
+            last_out[j, k] = piece[:, k * own_cols : (k + 1) * own_cols]
+            send(last_out.at[j, k], last_in.at[me], h_send.at[j * n_tp + k], h_recv.at[me], t, k)
+    cols = pl.ds(pl.multiple_of(z * chip_cols, chip_cols), chip_cols)
+    piece = dot(hidden, down2_v[:, cols]).astype(BF16)
+    for k in range(n_tp):
+        last_out[n_kv - 1, k] = piece[:, k * own_cols : (k + 1) * own_cols]
+    for i, k in enumerate(cores[1:]):
+        send(
+            last_out.at[n_kv - 1, k],
+            last_in.at[me],
+            h_send.at[(n_kv - 1) * n_tp + i],
+            h_recv.at[me],
+            z,
+            k,
+        )
+    summed = last_out[n_kv - 1, c].astype(F32)
+    for t, k in order[1:]:
+        who = t * n_tp + k
+        arrived(last_in.at[who], h_send.at[0], h_recv.at[who], t, k)
+        summed += last_in[who].astype(F32)
+    out_ref[...] = (after_v[c] + 0.5 * summed).astype(BF16)
+
+    store.wait()
+    for copy in sent:
+        copy.wait_send()
 
 
 def half_block(stream, norm_gain, w_gate, w_up, w_down):
@@ -23,7 +352,7 @@
     return (stream.astype(jnp.float32) + 0.5 * summed).astype(jnp.bfloat16)
 
 
-def body(
+def portable_body(
     stream,
     old_state,
     decay_amounts,
@@ -67,7 +396,7 @@
             jnp.sum(wide_cols * wide_cols, axis=1), "kv", scatter_dimension=0, tiled=True
         ),
     )
-    row_scale = lax.rsqrt(own_squares / D + EPSILON)[:, None]
+    row_scale = lax.rsqrt(own_squares / first_gain.shape[0] + EPSILON)[:, None]
     query = (query_sum * row_scale * key_dim ** (-0.5)).reshape(local_rows, local_heads, key_dim)
     keys = (key_sum * row_scale).reshape(local_rows, local_heads, key_dim)
     gate_logits = (decay_sum * row_scale).reshape(local_rows, local_heads, key_dim)
@@ -101,6 +430,127 @@
     return (mixed_stream, new_state)
 
 
+def body(n_kv, n_tp, *args):
+    (
+        stream,
+        old_state,
+        decay_amounts,
+        first_gain,
+        first_gate,
+        first_up,
+        first_down,
+        mixer_gain,
+        query_weight,
+        key_weight,
+        decay_weight,
+        value_weight,
+        output_gate_weight,
+        head_gain,
+        output_weight,
+        second_gain,
+        second_gate,
+        second_up,
+        second_down,
+    ) = args
+    seqs, own_cols = stream.shape
+    chip_cols = own_cols * n_tp
+    rows, heads, key_dim, value_dim = old_state.shape
+    if own_cols % 128 or value_dim % 128 or 3 * rows > 128 or n_kv * n_tp > 16:
+        return portable_body(*args)
+    proj_cols = 3 * heads * key_dim + 2 * heads * value_dim
+    n = n_kv * n_tp
+    first_gain, mixer_gain, head_gain, second_gain = (
+        g.reshape(1, -1) for g in (first_gain, mixer_gain, head_gain, second_gain)
+    )
+
+    def like(array):
+        return pltpu.VMEM(array.shape, array.dtype)
+
+    dma = pltpu.SemaphoreType.DMA
+    scratch = [
+        like(stream),
+        like(old_state),
+        like(decay_amounts),
+        like(first_gain),
+        like(first_gate),
+        like(first_up),
+        like(first_down),
+        like(mixer_gain),
+        pltpu.VMEM((chip_cols, proj_cols), BF16),
+        like(head_gain),
+        like(output_weight),
+        like(second_gain),
+        like(second_gate),
+        like(second_up),
+        like(second_down),
+        like(old_state),
+        pltpu.VMEM((n, seqs, own_cols), BF16),
+        pltpu.VMEM((n_kv, seqs, chip_cols), BF16),
+        pltpu.VMEM((n, seqs, chip_cols), BF16),
+        pltpu.VMEM((n_kv, seqs, chip_cols), BF16),
+        pltpu.VMEM((n_kv, rows, proj_cols + 128), F32),
+        pltpu.VMEM((n_kv, rows, proj_cols + 128), F32),
+        pltpu.VMEM((n_kv, rows, heads * value_dim), F32),
+        pltpu.VMEM((n, seqs, chip_cols), BF16),
+        pltpu.VMEM((n_tp, seqs, own_cols), F32),
+        pltpu.VMEM((n_kv, n_tp, seqs, own_cols), BF16),
+        pltpu.VMEM((n, seqs, own_cols), BF16),
+        dma((19,)),
+        dma,
+        dma((n,)),
+        dma((n,)),
+        dma((n,)),
+        dma((n,)),
+        dma((n_kv,)),
+        dma((n_kv,)),
+        dma((n_kv,)),
+        dma((n_kv,)),
+        dma((n_kv,)),
+        dma((n_kv,)),
+        dma((n,)),
+        dma((n,)),
+        dma((n,)),
+        dma((n,)),
+    ]
+    return pl.pallas_call(
+        functools.partial(layer_kernel, n_kv, n_tp),
+        out_shape=(
+            jax.ShapeDtypeStruct(stream.shape, stream.dtype),
+            jax.ShapeDtypeStruct(old_state.shape, old_state.dtype),
+        ),
+        in_specs=[pl.BlockSpec(memory_space=pl.ANY)] * 19,
+        out_specs=(
+            pl.BlockSpec(memory_space=pltpu.VMEM),
+            pl.BlockSpec(memory_space=pl.ANY),
+        ),
+        scratch_shapes=scratch,
+        compiler_params=pltpu.CompilerParams(
+            collective_id=0, has_side_effects=True, vmem_limit_bytes=60 * 1024 * 1024
+        ),
+        name="layer",
+    )(
+        stream,
+        old_state,
+        decay_amounts,
+        first_gain,
+        first_gate,
+        first_up,
+        first_down,
+        mixer_gain,
+        query_weight,
+        key_weight,
+        decay_weight,
+        value_weight,
+        output_gate_weight,
+        head_gain,
+        output_weight,
+        second_gain,
+        second_gate,
+        second_up,
+        second_down,
+    )
+
+
 def solution(mesh):
     in_specs = (
         P("dp", ("kv", "tp")),
@@ -124,4 +574,10 @@
         P(("kv", "tp"), None),
     )
     out_specs = (P("dp", ("kv", "tp")), P(("dp", "kv"), "tp", None, None))
-    return jax.shard_map(body, mesh=mesh, in_specs=in_specs, out_specs=out_specs, check_vma=False)
+    return jax.shard_map(
+        functools.partial(body, mesh.shape["kv"], mesh.shape["tp"]),
+        mesh=mesh,
+        in_specs=in_specs,
+        out_specs=out_specs,
+        check_vma=False,
+    )

time: 172 us -> 49.9 us (0.29)
  waiting for transfers between devices: 68.8 us -> 0 us
  blocking collectives: 60.8 us -> 0 us
  Pallas kernels: 0 us -> 30.8 us
  matrix products: 21.3 us -> 0 us
  local copies, waits for them, and re-layouts: 1.01 us -> 18.2 us
  between operations: 14.6 us -> 0.65 us
  other arithmetic: 4.73 us -> 0 us
    reduce_scatter x3 -> x0, waiting for transfers between devices: 68.8 us -> none  [the longest x2 62.4 us: half_block(): lax.psum_scatter(partial_out, ('kv', 'tp'), scatter_dimension=1, tiled=True)]
    all_gather x4 -> x0, blocking collectives: 44.1 us -> none  [the longest x2 30.4 us: half_block(): lax.all_gather(stream, ('kv', 'tp'), axis=1, tiled=True).astype(jnp.float32)]
    pallas_call x0 -> x1, Pallas kernels: none -> 30.8 us  [body(): pl.pallas_call(functools.partial(layer_kernel, n_kv, n_tp), out_shape=(ja...]
    dot_general x11 -> x0, matrix products: 21.3 us -> none  [the longest x2 9.16 us: half_block(): partial_out = jnp.dot(hidden, w_down, preferred_element_type=jnp.float32)]
    unnamed x22 -> x10, local copies, waits for them, and re-layouts: 0.66 us -> 18.2 us
    unnamed x1 -> x0, blocking collectives: 16.6 us -> none
    convert_element_type x3 -> x0, other arithmetic: 2.67 us -> none  [the longest x2 1.99 us: half_block(): return (stream.astype(jnp.float32) + 0.5 * summed).astype(jnp.bfloat16)]
  transfers between devices with their start and end apart: 3 -> 0, of which waited for: 3 -> 0; matrix products, arithmetic and copies ran while one was open for 0% -> 0% of each run, Pallas kernels for 0% -> 0%
where the time goes in v1:
time: 49.9 us; the launch traced here: 49.6 us
  Pallas kernels  30.8 us (62%)
  local copies, waits for them, and re-layouts  18.2 us (36%)
  between operations  0.65 us (1%)
    pallas_call x1, Pallas kernels, body(): pl.pallas_call(functools.partial(layer_kernel, n_kv, n_tp), out_shape=(ja...  30.8 us
    unnamed x10, local copies, waits for them, and re-layouts  18.2 us

profile of v1, /device:TPU:0, one launch (start us, length us, event | category | flops | bytes accessed | tf_op | source)
XLA Modules:
  0.0 49.6 jit_solution(6593178380430335004)
XLA Ops:
  0.6 0.0 copy-start
  0.6 4.8 %copy.21.gate1_h = bf16[2048,704]{1,0:T(8,128)(2,1)} copy(bf16[2048,704]{0,1:T(8,128)(2,1)} %param.23) | data formatting | bytes 5767168 | tf_op args[4]
  5.4 0.0 copy-done
  5.4 2.8 %copy.22.up1_h = bf16[2048,704]{1,0:T(8,128)(2,1)} copy(bf16[2048,704]{0,1:T(8,128)(2,1)S(1)} %copy-done) | data formatting | bytes 5767168 | tf_op args[5]
  8.2 0.0 copy-start.1
  8.2 4.8 %copy.23.gate2_h = bf16[2048,704]{1,0:T(8,128)(2,1)} copy(bf16[2048,704]{0,1:T(8,128)(2,1)} %param.35) | data formatting | bytes 5767168 | tf_op args[16]
  13.0 0.0 copy-done.1
  13.1 2.8 %copy.24.up2_h = bf16[2048,704]{1,0:T(8,128)(2,1)} copy(bf16[2048,704]{0,1:T(8,128)(2,1)S(1)} %copy-done.1) | data formatting | bytes 5767168 | tf_op args[17]
  15.9 30.8 %layer.1 = (bf16[8,256]{1,0:T(8,128)(2,1)}, f32[2,4,64,128]{3,2,1,0:T(8,128)}) custom-call(bf16[8,256]{1,0:T(8,128)(2,1)} %stream_h.1, f32[2,4,64,128]{3,2,1,0:T(8,128)} %state_h.1, f32[2,256]{1,0:T(2,128)} %amounts_h.1, f32[1,2048]{1,0:T(1,128)} %bitcast.4, bf16[2048,704]{1,0:T(8,128)(2,1)} %copy.21.gate1_h, bf16[2048,704]{1,0:T(8,128)(2,1)} %copy.22.up1_h, ...), custom_call_target="tpu_custom_call" | custom-call | tf_op jit(solution)/shard_map/layer/pallas_call | solution.py:515
  46.7 1.3 %copy.27 = bf16[8,256]{1,0:T(8,128)(2,1)} copy(bf16[8,256]{1,0:T(8,128)(2,1)} %get-tuple-element.4) | data formatting | bytes 8192
  47.9 1.7 %copy.28 = f32[2,4,64,128]{3,2,1,0:T(8,128)} copy(f32[2,4,64,128]{3,2,1,0:T(8,128)} %get-tuple-element.5) | data formatting | bytes 524288
Async XLA Ops:
  0.6 4.8 %copy-start = (bf16[2048,704]{0,1:T(8,128)(2,1)S(1)}, bf16[2048,704]{0,1:T(8,128)(2,1)}, u32[]{:S(2)}) copy-start(bf16[2048,704]{0,1:T(8,128)(2,1)} %param.24) | copy-start | bytes 8650756
  8.2 4.8 %copy-start.1 = (bf16[2048,704]{0,1:T(8,128)(2,1)S(1)}, bf16[2048,704]{0,1:T(8,128)(2,1)}, u32[]{:S(2)}) copy-start(bf16[2048,704]{0,1:T(8,128)(2,1)} %param.36) | copy-start | bytes 8650756

commit v2 on v1

--- a/solution.py
+++ b/solution.py
@@ -16,6 +16,10 @@
 
 def dot(a, b):
     return jnp.dot(a, b, preferred_element_type=F32)
+
+
+def dot_t(a, b):
+    return lax.dot_general(a, b, (((1,), (1,)), ((), ())), preferred_element_type=F32)
 
 
 def layer_kernel(
@@ -41,7 +45,7 @@
     up2_h,
     down2_h,
     out_ref,
-    newstate_h,
+    newstate_v,
     stream_v,
     state_v,
     amounts_v,
@@ -57,7 +61,6 @@
     gate2_v,
     up2_v,
     down2_v,
-    newstate_v,
     wide_v,
     down_out,
     down_in,
@@ -70,7 +73,6 @@
     last_out,
     last_in,
     load_sem,
-    store_sem,
     a_send,
     a_recv,
     c_send,
@@ -168,8 +170,8 @@
     load_gain1.wait()
     load_gate1.wait()
     load_up1.wait()
-    gate_acc = jnp.zeros((seqs, gate1_v.shape[1]), F32)
-    up_acc = jnp.zeros((seqs, up1_v.shape[1]), F32)
+    gate_acc = jnp.zeros((seqs, gate1_v.shape[0]), F32)
+    up_acc = jnp.zeros((seqs, up1_v.shape[0]), F32)
     squares = jnp.zeros((seqs, 1), F32)
     order = [(z, k) for k in cores] + [(t, k) for t in far[::-1] for k in cores]
     for i, (t, k) in enumerate(order):
@@ -180,8 +182,8 @@
         cols = pl.ds(pl.multiple_of(who * own_cols, own_cols), own_cols)
         scaled = (block * gain1_v[:, cols]).astype(BF16)
         squares += jnp.sum(block * block, axis=1, keepdims=True)
-        gate_acc += dot(scaled, gate1_v[cols, :])
-        up_acc += dot(scaled, up1_v[cols, :])
+        gate_acc += dot_t(scaled, gate1_v[:, cols])
+        up_acc += dot_t(scaled, up1_v[:, cols])
     scale = lax.rsqrt(squares / width + EPSILON)
     hidden = (jax.nn.silu(gate_acc * scale) * (up_acc * scale)).astype(BF16)
 
@@ -266,12 +268,10 @@
             )
             pieces.append(normed * gated[b : b + 1, lane])
         mixed_rows.append(jnp.concatenate(pieces, axis=1))
-    store = pltpu.make_async_copy(newstate_v, newstate_h, store_sem)
 
     mixed_v[z] = jnp.concatenate(mixed_rows, axis=0).astype(BF16).astype(F32)
     for j, t in enumerate(far):
         send(mixed_v.at[z], mixed_v.at[z], e_send.at[j], e_recv.at[z], t, c)
-    store.start()
     load_output.wait()
     for t in far[::-1]:
         arrived(mixed_v.at[t], e_send.at[0], e_recv.at[t], t, c)
@@ -282,8 +282,8 @@
         send(attn_v.at[me], attn_v.at[me], g_send.at[p], g_recv.at[me], t, k)
     for copy in load_second:
         copy.wait()
-    gate_acc = jnp.zeros((seqs, gate2_v.shape[1]), F32)
-    up_acc = jnp.zeros((seqs, up2_v.shape[1]), F32)
+    gate_acc = jnp.zeros((seqs, gate2_v.shape[0]), F32)
+    up_acc = jnp.zeros((seqs, up2_v.shape[0]), F32)
     squares = jnp.zeros((seqs, 1), F32)
     for t in [z] + far[::-1]:
         if t is not z:
@@ -302,8 +302,8 @@
         cols = pl.ds(pl.multiple_of(t * chip_cols, chip_cols), chip_cols)
         scaled = (block * gain2_v[:, cols]).astype(BF16)
         squares += jnp.sum(block * block, axis=1, keepdims=True)
-        gate_acc += dot(scaled, gate2_v[cols, :])
-        up_acc += dot(scaled, up2_v[cols, :])
+        gate_acc += dot_t(scaled, gate2_v[:, cols])
+        up_acc += dot_t(scaled, up2_v[:, cols])
     scale = lax.rsqrt(squares / width + EPSILON)
     hidden = (jax.nn.silu(gate_acc * scale) * (up_acc * scale)).astype(BF16)
 
@@ -334,7 +334,6 @@
         summed += last_in[who].astype(F32)
     out_ref[...] = (after_v[c] + 0.5 * summed).astype(BF16)
 
-    store.wait()
     for copy in sent:
         copy.wait_send()
 
@@ -463,6 +462,10 @@
         g.reshape(1, -1) for g in (first_gain, mixer_gain, head_gain, second_gain)
     )
 
+    first_gate, first_up, second_gate, second_up = (
+        w.T for w in (first_gate, first_up, second_gate, second_up)
+    )
+
     def like(array):
         return pltpu.VMEM(array.shape, array.dtype)
 
@@ -483,7 +486,6 @@
         like(second_gate),
         like(second_up),
         like(second_down),
-        like(old_state),
         pltpu.VMEM((n, seqs, own_cols), BF16),
         pltpu.VMEM((n_kv, seqs, chip_cols), BF16),
         pltpu.VMEM((n, seqs, chip_cols), BF16),
@@ -496,7 +498,6 @@
         pltpu.VMEM((n_kv, n_tp, seqs, own_cols), BF16),
         pltpu.VMEM((n, seqs, own_cols), BF16),
         dma((19,)),
-        dma,
         dma((n,)),
         dma((n,)),
         dma((n,)),
@@ -515,13 +516,13 @@
     return pl.pallas_call(
         functools.partial(layer_kernel, n_kv, n_tp),
         out_shape=(
-            jax.ShapeDtypeStruct(stream.shape, stream.dtype),
-            jax.ShapeDtypeStruct(old_state.shape, old_state.dtype),
+            pltpu.VMEM(stream.shape, stream.dtype),
+            pltpu.VMEM(old_state.shape, old_state.dtype),
         ),
         in_specs=[pl.BlockSpec(memory_space=pl.ANY)] * 19,
         out_specs=(
             pl.BlockSpec(memory_space=pltpu.VMEM),
-            pl.BlockSpec(memory_space=pl.ANY),
+            pl.BlockSpec(memory_space=pltpu.VMEM),
         ),
         scratch_shapes=scratch,
         compiler_params=pltpu.CompilerParams(

time: 49.9 us -> 33.3 us (0.67)
  local copies, waits for them, and re-layouts: 18.2 us -> 1.3 us
    unnamed x10 -> x2, local copies, waits for them, and re-layouts: 18.2 us -> 1.3 us
where the time goes in v2:
time: 33.3 us; the launch traced here: 33.1 us
  Pallas kernels  31.2 us (94%)
  local copies, waits for them, and re-layouts  1.3 us (4%)
  between operations  0.65 us (2%)
    pallas_call x1, Pallas kernels, body(): pl.pallas_call(functools.partial(layer_kernel, n_kv, n_tp), out_shape=(pl...  31.2 us
    unnamed x2, local copies, waits for them, and re-layouts  1.3 us

profile of v2, /device:TPU:0, one launch (start us, length us, event | category | flops | bytes accessed | tf_op | source)
XLA Modules:
  0.0 33.1 jit_solution(4150779469755193126)
XLA Ops:
  0.6 31.2 %layer.1 = (bf16[8,256]{1,0:T(8,128)(2,1)S(1)}, f32[2,4,64,128]{3,2,1,0:T(8,128)S(1)}) custom-call(bf16[8,256]{1,0:T(8,128)(2,1)} %stream_h.1, f32[2,4,64,128]{3,2,1,0:T(8,128)} %state_h.1, f32[2,256]{1,0:T(2,128)} %amounts_h.1, f32[1,2048]{1,0:T(1,128)} %bitcast.12, bf16[704,2048]{1,0:T(8,128)(2,1)} %bitcast.8, bf16[704,2048]{1,0:T(8,128)(2,1)} %bitcast.9, ...), custom_call_target="tpu_custom_call" | custom-call | tf_op jit(solution)/shard_map/layer/pallas_call | solution.py:516
  31.8 0.6 %copy.23 = bf16[8,256]{1,0:T(8,128)(2,1)} copy(bf16[8,256]{1,0:T(8,128)(2,1)S(1)} %get-tuple-element.2) | data formatting | bytes 8192
  32.4 0.7 %copy.24 = f32[2,4,64,128]{3,2,1,0:T(8,128)} copy(f32[2,4,64,128]{3,2,1,0:T(8,128)S(1)} %get-tuple-element.3) | data formatting | bytes 524288

commit v3 on v2

--- a/solution.py
+++ b/solution.py
@@ -162,7 +162,6 @@
     for ref in (query_h, key_h, decay_h, value_h, outgate_h):
         load_mix.append(load(ref, proj_v.at[:, at : at + ref.shape[1]]))
         at += ref.shape[1]
-    proj_cols = at
     load_output = load(output_h, output_v)
     load_second = [load(gain2_h, gain2_v), load(gate2_h, gate2_v), load(up2_h, up2_v)]
     load_down2 = load(down2_h, down2_v)
@@ -220,62 +219,71 @@
     scaled = (middle_wide * mixgain_v[...]).astype(BF16)
     part = dot(scaled, proj_v[...])
     square_part = jnp.broadcast_to(
-        jnp.sum(middle_wide * middle_wide, axis=1, keepdims=True), (seqs, 128)
-    )
+        jnp.sum(middle_wide * middle_wide, axis=1, keepdims=True), (seqs, key_cols)
+    )
+    queries_keys = part[:, : 2 * key_cols]
+    logits_squares = jnp.concatenate([part[:, 2 * key_cols : 3 * key_cols], square_part], axis=1)
+    values_part = part[:, 3 * key_cols : 3 * key_cols + value_cols]
+    gates_part = part[:, 3 * key_cols + value_cols :]
     for j in range(n_kv):
-        proj_out[j, :, :proj_cols] = part[j * rows : (j + 1) * rows]
-        proj_out[j, :, proj_cols:] = square_part[j * rows : (j + 1) * rows]
+        mine = slice(j * rows, (j + 1) * rows)
+        proj_out[j] = jnp.concatenate(
+            [queries_keys[mine], logits_squares[mine], values_part[mine], gates_part[mine]], axis=0
+        )
     for j, t in enumerate(far):
         send(proj_out.at[t], proj_in.at[z], d_send.at[j], d_recv.at[z], t, c)
     for j, t in enumerate(far):
         send(middle_v.at[z], middle_v.at[z], m_send.at[j], m_recv.at[z], t, c)
 
+    for copy in load_small:
+        copy.wait()
+    load_state.wait()
+    load_output.wait()
     total = proj_out[z]
     for t in far[::-1]:
         arrived(proj_in.at[t], d_send.at[0], d_recv.at[t], t, c)
         total += proj_in[t]
-    scale = lax.rsqrt(total[:, proj_cols : proj_cols + 1] / width + EPSILON)
-    total = total[:, :proj_cols] * scale
-    query = total[:, :key_cols] * key_dim ** (-0.5)
-    keys = total[:, key_cols : 2 * key_cols]
-    logits = total[:, 2 * key_cols : 3 * key_cols]
-    values = total[:, 3 * key_cols : 3 * key_cols + value_cols]
-    outgate = total[:, 3 * key_cols + value_cols :]
-    for copy in load_small:
-        copy.wait()
+    scale = lax.rsqrt(total[rows : 2 * rows, key_cols : key_cols + 1] / width + EPSILON)
+    query = total[:rows, :key_cols] * (scale * key_dim ** (-0.5))
+    keys = total[:rows, key_cols:] * scale
+    logits = total[rows : 2 * rows, :key_cols] * scale
+    values = total[2 * rows : 3 * rows] * scale
+    outgate = total[3 * rows :] * scale
     log_sigmoid = jnp.minimum(logits, 0.0) - jnp.log(1.0 + jnp.exp(-jnp.abs(logits)))
     decay = jnp.exp(log_sigmoid / GATE_SOFTNESS - amounts_v[...])
     stacked = jnp.concatenate(
-        [query, keys, decay, jnp.zeros((128 - 3 * rows, key_cols), F32)], axis=0
+        [query, keys, decay, jnp.zeros((-3 * rows % 8, key_cols), F32)], axis=0
     )
     turned = stacked.T
     gated = headgain_v[...] * jax.nn.silu(outgate)
-    load_state.wait()
-    mixed_rows = []
-    for b in range(rows):
-        pieces = []
-        for h in range(heads):
-            span = slice(h * key_dim, (h + 1) * key_dim)
-            lane = slice(h * value_dim, (h + 1) * value_dim)
+    readouts, gates = [], []
+    for h in range(heads):
+        span = slice(h * key_dim, (h + 1) * key_dim)
+        lane = slice(h * value_dim, (h + 1) * value_dim)
+        gates.append(gated[:, lane])
+        for b in range(rows):
             q_col = turned[span, b : b + 1]
             k_col = turned[span, rows + b : rows + b + 1]
             d_col = turned[span, 2 * rows + b : 2 * rows + b + 1]
             new = d_col * state_v[b, h] + k_col * values[b : b + 1, lane]
             newstate_v[b, h] = new
-            readout = jnp.sum(q_col * new, axis=0, keepdims=True)
-            normed = readout * lax.rsqrt(
-                jnp.mean(readout * readout, axis=1, keepdims=True) + EPSILON
-            )
-            pieces.append(normed * gated[b : b + 1, lane])
-        mixed_rows.append(jnp.concatenate(pieces, axis=1))
-
-    mixed_v[z] = jnp.concatenate(mixed_rows, axis=0).astype(BF16).astype(F32)
+            readouts.append(jnp.sum(q_col * new, axis=0, keepdims=True))
+    readout = jnp.concatenate(readouts, axis=0)
+    normed = readout * lax.rsqrt(jnp.mean(readout * readout, axis=1, keepdims=True) + EPSILON)
+
+    mixed_v[z] = (normed * jnp.concatenate(gates, axis=0)).astype(BF16).astype(F32)
     for j, t in enumerate(far):
         send(mixed_v.at[z], mixed_v.at[z], e_send.at[j], e_recv.at[z], t, c)
-    load_output.wait()
     for t in far[::-1]:
         arrived(mixed_v.at[t], e_send.at[0], e_recv.at[t], t, c)
-    mixed = jnp.concatenate([mixed_v[j] for j in range(n_kv)], axis=0).astype(BF16)
+    blocks = [mixed_v[j] for j in range(n_kv)]
+    mixed = jnp.concatenate(
+        [
+            jnp.concatenate([block[h * rows : (h + 1) * rows] for block in blocks], axis=0)
+            for h in range(heads)
+        ],
+        axis=1,
+    ).astype(BF16)
     attn_v[me] = dot(mixed, output_v[...]).astype(BF16)
 
     for p, (t, k) in enumerate(peers):
@@ -336,6 +344,17 @@
 
     for copy in sent:
         copy.wait_send()
+
+
+def store_kernel(stream_v, state_v, stream_h, state_h, sem):
+    copies = [
+        pltpu.make_async_copy(state_v, state_h, sem.at[0]),
+        pltpu.make_async_copy(stream_v, stream_h, sem.at[1]),
+    ]
+    for copy in copies:
+        copy.start()
+    for copy in copies:
+        copy.wait()
 
 
 def half_block(stream, norm_gain, w_gate, w_up, w_down):
@@ -454,7 +473,7 @@
     seqs, own_cols = stream.shape
     chip_cols = own_cols * n_tp
     rows, heads, key_dim, value_dim = old_state.shape
-    if own_cols % 128 or value_dim % 128 or 3 * rows > 128 or n_kv * n_tp > 16:
+    if own_cols % 128 or value_dim != 2 * key_dim or value_dim % 128 or n_kv * n_tp > 16:
         return portable_body(*args)
     proj_cols = 3 * heads * key_dim + 2 * heads * value_dim
     n = n_kv * n_tp
@@ -490,9 +509,9 @@
         pltpu.VMEM((n_kv, seqs, chip_cols), BF16),
         pltpu.VMEM((n, seqs, chip_cols), BF16),
         pltpu.VMEM((n_kv, seqs, chip_cols), BF16),
-        pltpu.VMEM((n_kv, rows, proj_cols + 128), F32),
-        pltpu.VMEM((n_kv, rows, proj_cols + 128), F32),
-        pltpu.VMEM((n_kv, rows, heads * value_dim), F32),
+        pltpu.VMEM((n_kv, 4 * rows, heads * value_dim), F32),
+        pltpu.VMEM((n_kv, 4 * rows, heads * value_dim), F32),
+        pltpu.VMEM((n_kv, heads * rows, value_dim), F32),
         pltpu.VMEM((n, seqs, chip_cols), BF16),
         pltpu.VMEM((n_tp, seqs, own_cols), F32),
         pltpu.VMEM((n_kv, n_tp, seqs, own_cols), BF16),
@@ -513,7 +532,7 @@
         dma((n,)),
         dma((n,)),
     ]
-    return pl.pallas_call(
+    mixed_stream, new_state = pl.pallas_call(
         functools.partial(layer_kernel, n_kv, n_tp),
         out_shape=(
             pltpu.VMEM(stream.shape, stream.dtype),
@@ -550,6 +569,20 @@
         second_up,
         second_down,
     )
+    return pl.pallas_call(
+        store_kernel,
+        out_shape=(
+            jax.ShapeDtypeStruct(stream.shape, stream.dtype),
+            jax.ShapeDtypeStruct(old_state.shape, old_state.dtype),
+        ),
+        in_specs=[pl.BlockSpec(memory_space=pltpu.VMEM)] * 2,
+        out_specs=(pl.BlockSpec(memory_space=pl.ANY),) * 2,
+        scratch_shapes=[dma((2,))],
+        name="store",
+    )(
+        pltpu.with_memory_space_constraint(mixed_stream, pltpu.VMEM),
+        pltpu.with_memory_space_constraint(new_state, pltpu.VMEM),
+    )
 
 
 def solution(mesh):

time: 33.3 us -> 32.3 us (0.970)
  local copies, waits for them, and re-layouts: 1.3 us -> 0 us
    unnamed x2 -> x0, local copies, waits for them, and re-layouts: 1.3 us -> none
    pallas_call x0 -> x1, Pallas kernels: none -> 0.72 us  [body(): pl.pallas_call(store_kernel, out_shape=(jax.ShapeDtypeStruct(stream.shape...]
    pallas_call x1, Pallas kernels: 31.2 us -> 30.8 us  [body(): pl.pallas_call(functools.partial(layer_kernel, n_kv, n_tp), out_shape=(pl...]
where the time goes in v3:
time: 32.3 us; the launch traced here: 32.2 us
  Pallas kernels  31.5 us (98%)
  between operations  0.65 us (2%)
    pallas_call x1, Pallas kernels, body(): pl.pallas_call(functools.partial(layer_kernel, n_kv, n_tp), out_shape=(pl...  30.8 us
    pallas_call x1, Pallas kernels, body(): pl.pallas_call(store_kernel, out_shape=(jax.ShapeDtypeStruct(stream.shape...  0.72 us

profile of v3, /device:TPU:0, one launch (start us, length us, event | category | flops | bytes accessed | tf_op | source)
XLA Modules:
  0.0 32.2 jit_solution(3432372541188082455)
XLA Ops:
  0.6 30.8 %layer.1 = (bf16[8,256]{1,0:T(8,128)(2,1)S(1)}, f32[2,4,64,128]{3,2,1,0:T(8,128)S(1)}) custom-call(bf16[8,256]{1,0:T(8,128)(2,1)} %stream_h.1, f32[2,4,64,128]{3,2,1,0:T(8,128)} %state_h.1, f32[2,256]{1,0:T(2,128)} %amounts_h.1, f32[1,2048]{1,0:T(1,128)} %bitcast.12, bf16[704,2048]{1,0:T(8,128)(2,1)} %bitcast.8, bf16[704,2048]{1,0:T(8,128)(2,1)} %bitcast.9, ...), custom_call_target="tpu_custom_call" | custom-call | tf_op jit(solution)/shard_map/layer/pallas_call | solution.py:535
  31.5 0.7 %store.1 = (bf16[8,256]{1,0:T(8,128)(2,1)}, f32[2,4,64,128]{3,2,1,0:T(8,128)}) custom-call(bf16[8,256]{1,0:T(8,128)(2,1)S(1)} %get-tuple-element.4.stream_v, f32[2,4,64,128]{3,2,1,0:T(8,128)S(1)} %get-tuple-element.5.state_v), custom_call_target="tpu_custom_call" | custom-call | tf_op jit(solution)/shard_map/store/pallas_call | solution.py:572

commit v4 on v3

--- a/solution.py
+++ b/solution.py
@@ -107,10 +107,6 @@
         return copy
 
     load_stream = load(stream_h, stream_v)
-    load_gain1 = load(gain1_h, gain1_v)
-    load_gate1 = load(gate1_h, gate1_v)
-    load_up1 = load(up1_h, up1_v)
-    load_down1 = load(down1_h, down1_v)
 
     far = []
     for j in range(n_kv - 1):
@@ -124,6 +120,10 @@
     barrier = pltpu.get_barrier_semaphore()
     for t, k in peers:
         pl.semaphore_signal(barrier, inc=1, device_id={"kv": t, "tp": k}, device_id_type=MESH)
+    load_gain1 = load(gain1_h, gain1_v)
+    load_gate1 = load(gate1_h, gate1_v)
+    load_up1 = load(up1_h, up1_v)
+    load_down1 = load(down1_h, down1_v)
     pl.semaphore_wait(barrier, len(peers))
 
     sent = []

time: 32.3 us -> 32.3 us (level)
  no operation moved by 1% of the time
where the time goes in v4:
time: 32.3 us; the launch traced here: 32.2 us
  Pallas kernels  31.5 us (98%)
  between operations  0.65 us (2%)
    pallas_call x1, Pallas kernels, body(): pl.pallas_call(functools.partial(layer_kernel, n_kv, n_tp), out_shape=(pl...  30.8 us
    pallas_call x1, Pallas kernels, body(): pl.pallas_call(store_kernel, out_shape=(jax.ShapeDtypeStruct(stream.shape...  0.72 us

profile of v4, /device:TPU:0, one launch (start us, length us, event | category | flops | bytes accessed | tf_op | source)
XLA Modules:
  0.0 32.2 jit_solution(2795027783002850572)
XLA Ops:
  0.6 30.8 %layer.1 = (bf16[8,256]{1,0:T(8,128)(2,1)S(1)}, f32[2,4,64,128]{3,2,1,0:T(8,128)S(1)}) custom-call(bf16[8,256]{1,0:T(8,128)(2,1)} %stream_h.1, f32[2,4,64,128]{3,2,1,0:T(8,128)} %state_h.1, f32[2,256]{1,0:T(2,128)} %amounts_h.1, f32[1,2048]{1,0:T(1,128)} %bitcast.12, bf16[704,2048]{1,0:T(8,128)(2,1)} %bitcast.8, bf16[704,2048]{1,0:T(8,128)(2,1)} %bitcast.9, ...), custom_call_target="tpu_custom_call" | custom-call | tf_op jit(solution)/shard_map/layer/pallas_call | solution.py:535
  31.5 0.7 %store.1 = (bf16[8,256]{1,0:T(8,128)(2,1)}, f32[2,4,64,128]{3,2,1,0:T(8,128)}) custom-call(bf16[8,256]{1,0:T(8,128)(2,1)S(1)} %get-tuple-element.4.stream_v, f32[2,4,64,128]{3,2,1,0:T(8,128)S(1)} %get-tuple-element.5.state_v), custom_call_target="tpu_custom_call" | custom-call | tf_op jit(solution)/shard_map/store/pallas_call | solution.py:572
